TPU v7x, 32 devices: a whole 2x2x4 slice. The times are simulated.
32 devices in a mesh: ep: 16 (over z, y, x), tp: 2 (over core).
Axes of the slice: x: 2, y: 2, z: 4, core: 2. Of those that a mesh axis runs over, the one named last changes fastest.
Arguments:
- tokens: bfloat16 [256, 2048], P('ep', 'tp'), may hold values from -6 to 6
- state: float32 [256, 4, 128, 128], P('ep', 'tp'), may hold values from -4 to 4
- norm_mix: float32 [2048], replicated, may hold values from 0.1 to 1.9
- w_query: bfloat16 [2048, 512], P(None, 'tp'), may hold values from -0.125 to 0.125
- w_key: bfloat16 [2048, 512], P(None, 'tp'), may hold values from -0.125 to 0.125
- w_value: bfloat16 [2048, 512], P(None, 'tp'), may hold values from -0.125 to 0.125
- w_out: bfloat16 [512, 2048], P('tp'), may hold values from -0.25 to 0.25
- norm_ffn: float32 [2048], P('tp'), may hold values from 0.1 to 1.9
- gate_vector: bfloat16 [2048], P('tp'), may hold values from -0.125 to 0.125
- dense_gate: bfloat16 [2048, 2816], P('tp', 'ep'), may hold values from -0.125 to 0.125
- dense_up: bfloat16 [2048, 2816], P('tp', 'ep'), may hold values from -0.125 to 0.125
- dense_down: bfloat16 [2816, 2048], P('ep', 'tp'), may hold values from -0.109375 to 0.109375
- exp_gate: bfloat16 [16, 2048, 1408], P('ep', None, 'tp'), may hold values from -0.125 to 0.125
- exp_up: bfloat16 [16, 2048, 1408], P('ep', None, 'tp'), may hold values from -0.125 to 0.125
- exp_down: bfloat16 [16, 1408, 2048], P('ep', 'tp'), may hold values from -0.109375 to 0.109375
- routes: int32 [256, 2], P('ep'), may hold values from 0 to 7, all different within a row; in each aligned block of 16 rows (0 to 15, 16 to 31, ...) at most 5 rows name the same one
- route_w: bfloat16 [256, 2], P('ep'), may hold values from 0.099609375 to 1
Outputs:
- mixed: bfloat16 [256, 2048], P('ep', 'tp')
- new_state: float32 [256, 4, 128, 128], P('ep', 'tp')
Inputs may be any that keep to these rules, and one draw needn't show every extreme that they name: `routes`: each row names 2 different experts. Within the rows of one device (aligned blocks of 16 rows) no expert is named by more than 5 rows, a bound that some blocks reach.
All inputs are finite; a program needn't handle non-finite values.
Results may differ from a plain program's by a relative error of at most 0.014.
Values may be sent and summed in bfloat16 or wider, within the bound.
A program may use at most 128 MiB of HBM per device.

v0:
```python
import jax
import jax.numpy as jnp
from jax import lax
from jax.sharding import PartitionSpec as P

EXPERTS = 8
CAP = 5


epsilon = 1e-06


def route_tables(routes, route_w):
    onehot = (routes[:, :, None] == jnp.arange(EXPERTS, dtype=jnp.int32)[None, None, :]).astype(
        jnp.float32
    )
    member = jnp.sum(onehot, axis=1)
    weight = jnp.sum(onehot * route_w.astype(jnp.float32)[:, :, None], axis=1)
    place = jnp.cumsum(member, axis=0) - member
    slot_ids = jnp.arange(CAP, dtype=jnp.float32)
    select = member.T[:, None, :] * (place.T[:, None, :] == slot_ids[None, :, None]).astype(
        jnp.float32
    )
    return (select, weight)


def expert_math(flat_rows, weights):
    gate_pre = jnp.dot(flat_rows, weights[0], preferred_element_type=jnp.float32)
    up_part = jnp.dot(flat_rows, weights[1], preferred_element_type=jnp.float32)
    hidden = (jax.nn.silu(gate_pre) * up_part).astype(jnp.bfloat16)
    return jnp.dot(hidden, weights[2], preferred_element_type=jnp.float32)


def expert_apply(slot_rows, weights):
    full_rows = lax.all_gather(slot_rows, "tp", axis=2, tiled=True)
    row_count = full_rows.shape[0] * full_rows.shape[1]
    partial_value = expert_math(full_rows.reshape(row_count, full_rows.shape[2]), weights)
    summed = lax.psum_scatter(
        partial_value.astype(jnp.bfloat16), "tp", scatter_dimension=1, tiled=True
    ).astype(jnp.float32)
    return summed.reshape(slot_rows.shape[0], slot_rows.shape[1], summed.shape[1])


def body(
    tokens,
    state,
    norm_mix,
    w_query,
    w_key,
    w_value,
    w_out,
    norm_ffn,
    gate_vector,
    dense_gate,
    dense_up,
    dense_down,
    exp_gate,
    exp_up,
    exp_down,
    routes,
    route_w,
):
    highest = lax.Precision.HIGHEST
    row_count, half_width = tokens.shape
    heads_here, head_size = (state.shape[1], state.shape[2])
    weights = (exp_gate[0], exp_up[0], exp_down[0])
    full_x = lax.all_gather(tokens, "tp", axis=1, tiled=True)
    width = full_x.shape[1]
    full_f = full_x.astype(jnp.float32)
    normed = (
        full_f
        * lax.rsqrt(jnp.sum(full_f * full_f, axis=1, keepdims=True) / width + epsilon)
        * norm_mix
    ).astype(jnp.bfloat16)
    query = jnp.dot(normed, w_query, preferred_element_type=jnp.float32).astype(jnp.bfloat16)
    key_rows = jnp.dot(normed, w_key, preferred_element_type=jnp.float32).astype(jnp.bfloat16)
    value_rows = jnp.dot(normed, w_value, preferred_element_type=jnp.float32).astype(jnp.bfloat16)
    query3 = query.astype(jnp.float32).reshape(row_count, heads_here, head_size)
    key3 = key_rows.astype(jnp.float32).reshape(row_count, heads_here, head_size) * head_size ** (
        -0.5
    )
    value3 = value_rows.astype(jnp.float32).reshape(row_count, heads_here, head_size)
    head_ids = (lax.axis_index("tp") * heads_here + jnp.arange(heads_here, dtype=jnp.int32)).astype(
        jnp.float32
    )
    decay = 1.0 - jnp.exp2(-3.0 - 2.0 * head_ids)
    new_state = decay[None, :, None, None] * state + jnp.einsum(
        "shd,she->shde", key3, value3, precision=highest
    )
    read = jnp.einsum("shd,shde->she", query3, new_state, precision=highest)
    centre = jnp.mean(read, axis=2, keepdims=True)
    spread = jnp.mean(jnp.square(read - centre), axis=2, keepdims=True)
    heads_out = (
        ((read - centre) * lax.rsqrt(spread + epsilon))
        .astype(jnp.bfloat16)
        .reshape(row_count, heads_here * head_size)
    )
    mix_part = jnp.dot(heads_out, w_out, preferred_element_type=jnp.float32)
    mix_half = lax.psum_scatter(
        mix_part.astype(jnp.bfloat16), "tp", scatter_dimension=1, tiled=True
    ).astype(jnp.float32)
    after = (tokens.astype(jnp.float32) + mix_half).astype(jnp.bfloat16)
    after_hf = after.astype(jnp.float32)
    squares = lax.psum(jnp.sum(after_hf * after_hf, axis=1, keepdims=True), "tp")
    after_f = after.astype(jnp.float32)
    normed2 = (after_f * lax.rsqrt(squares / width + epsilon) * norm_ffn).astype(jnp.bfloat16)
    all_rows = lax.all_gather(normed2, "ep", axis=0, tiled=True)
    dense_pre = jnp.dot(all_rows, dense_gate, preferred_element_type=jnp.float32)
    up_pre = jnp.dot(all_rows, dense_up, preferred_element_type=jnp.float32)
    logit = jnp.dot(all_rows, gate_vector, preferred_element_type=jnp.float32)
    dense_pre, up_pre, logit = (
        lax.psum(dense_pre.astype(jnp.bfloat16), "tp").astype(jnp.float32),
        lax.psum(up_pre.astype(jnp.bfloat16), "tp").astype(jnp.float32),
        lax.psum(logit.astype(jnp.bfloat16), "tp").astype(jnp.float32),
    )
    dense_hidden = (jax.nn.sigmoid(logit)[:, None] * jax.nn.silu(dense_pre) * up_pre).astype(
        jnp.bfloat16
    )
    ep_count = lax.axis_size("ep")
    group_size = ep_count // EXPERTS
    select, weight = route_tables(routes, route_w)
    outgoing = jnp.einsum(
        "ecr,rd->ecd", select.astype(jnp.bfloat16), normed2, preferred_element_type=jnp.float32
    ).astype(jnp.bfloat16)
    outgoing = jnp.repeat(outgoing, group_size, axis=0)
    served = expert_apply(
        lax.all_to_all(outgoing, "ep", split_axis=0, concat_axis=0, tiled=True), weights
    )
    returned = lax.all_to_all(
        served.astype(jnp.bfloat16), "ep", split_axis=0, concat_axis=0, tiled=True
    ).astype(served.dtype)
    per_expert = jnp.sum(returned.reshape(EXPERTS, group_size, CAP, half_width), axis=1)
    local_moe = jnp.einsum(
        "ecr,ecd->rd", select * weight.T[:, None, :], per_expert, precision=highest
    )
    value = jnp.dot(dense_hidden, dense_down, preferred_element_type=jnp.float32)
    combined = lax.psum_scatter(value, "ep", scatter_dimension=0, tiled=True)
    return ((after_f + local_moe + combined).astype(jnp.bfloat16), new_state)


def solution(mesh):
    return jax.shard_map(
        body,
        mesh=mesh,
        in_specs=(
            P("ep", "tp"),
            P("ep", "tp", None, None),
            P(),
            P(None, "tp"),
            P(None, "tp"),
            P(None, "tp"),
            P("tp", None),
            P("tp"),
            P("tp"),
            P("tp", "ep"),
            P("tp", "ep"),
            P("ep", "tp"),
            P("ep", None, "tp"),
            P("ep", None, "tp"),
            P("ep", "tp", None),
            P("ep", None),
            P("ep", None),
        ),
        out_specs=(P("ep", "tp"), P("ep", "tp", None, None)),
        check_vma=False,
    )
```

profile of v0, /device:TPU:0, one launch (start us, length us, event | category | flops | bytes accessed | tf_op | source)
XLA Modules:
  0.0 210.0 jit_solution(15320848404340629431)
XLA Ops:
  7.2 2.3 %all_gather.9 = bf16[16,2048]{1,0:T(8,128)(2,1)S(1)} all-gather(bf16[16,1024]{1,0:T(8,128)(2,1)} %param.17), channel_id=1, replica_groups=mesh['ep'=16,'tp'=2] {'tp'}, dimensions={1}, use_global_device_ids=true | all-gather | bytes 98304 | tf_op jit(solution)/shard_map/all_gather | solution.py:67
  9.7 1.5 convolution_convert_fusion.6
  11.3 1.5 fusion.18
  12.8 1.5 fusion.20
  14.4 2.0 multiply_add_fusion
  16.4 1.3 copy-done.1
  17.7 1.1 fusion.63
  18.9 0.2 multiply_reduce_fusion
  19.2 2.1 convolution_convert_fusion
  21.6 10.0 %reduce-scatter.4.cloned.1.call-done = bf16[16,1024]{1,0:T(8,128)(2,1)} async-done(((bf16[16,2048]{1,0:T(8,128)(2,1)}), bf16[16,1024]{1,0:T(8,128)(2,1)}) %reduce-scatter.4.cloned.1.call-update) | async-done | bytes 32784 | tf_op jit(solution)/shard_map/reduce_scatter | solution.py:99
  31.6 0.9 fusion.43
  32.5 2.5 %psum.28 = f32[16,1]{0,1:T(1,128)S(1)} all-reduce(f32[16,1]{0,1:T(1,128)S(1)} %bitcast.72), channel_id=1, replica_groups=mesh['ep'=16,'tp'=2] {'tp'}, use_global_device_ids=true, to_apply=%region_8.0 | all-reduce | flops 16 | bytes 128 | tf_op jit(solution)/shard_map/psum | solution.py:104
  35.0 0.8 fusion.45
  35.8 44.0 %all_gather.11 = bf16[256,1024]{1,0:T(8,128)(2,1)S(1)} all-gather(bf16[16,1024]{1,0:T(8,128)(2,1)S(1)} %fusion.45), channel_id=1, replica_groups=mesh['ep'=16,'tp'=2] {'ep'}, dimensions={0}, use_global_device_ids=true | all-gather | bytes 557056 | tf_op jit(solution)/shard_map/all_gather | solution.py:107
  79.8 0.1 convolution_convert_fusion.3
  80.0 0.7 broadcast_in_dim.5
  80.7 4.2 %all-to-all-start = ((bf16[16,5,1024]{2,1,0:T(8,128)(2,1)}), bf16[16,5,1024]{2,1,0:T(8,128)(2,1)}, u32[]{:S(2)}, u32[]{:S(2)}) async-start(bf16[16,5,1024]{2,1,0:T(8,128)(2,1)} %bitcast.63), calls=%async_computation.1 | async-start | bytes 524288 | tf_op jit(solution)/shard_map/all_to_all | solution.py:127
  84.9 1.9 convolution_convert_fusion.1
  86.9 2.0 convolution_convert_fusion.2
  88.9 4.5 %all-to-all-done = bf16[16,5,1024]{2,1,0:T(8,128)(2,1)} async-done(((bf16[16,5,1024]{2,1,0:T(8,128)(2,1)}), bf16[16,5,1024]{2,1,0:T(8,128)(2,1)}, u32[]{:S(2)}, u32[]{:S(2)}) %all-to-all-start) | async-done | bytes 163872 | tf_op jit(solution)/shard_map/all_to_all | solution.py:127
  93.4 3.8 %all_gather.10 = bf16[16,5,2048]{2,1,0:T(8,128)(2,1)} all-gather(bf16[16,5,1024]{2,1,0:T(8,128)(2,1)} %all-to-all-done), channel_id=1, replica_groups=mesh['ep'=16,'tp'=2] {'tp'}, dimensions={2}, use_global_device_ids=true | all-gather | bytes 491520 | tf_op jit(solution)/shard_map/all_gather | solution.py:35
  97.2 1.9 reshape.74
  99.1 3.6 %fusion.4 = f32[80,704]{1,0:T(8,128)} fusion(bf16[80,2048]{1,0:T(8,128)(2,1)} %reshape.74, bf16[1,2048,704]{1,2,0:T(8,128)(2,1)} %param.29), kind=kOutput, calls=%fused_computation.4 | convolution fusion | flops 230686720 | bytes 3436544 | tf_op jit(solution)/shard_map/dot_general | solution.py:28
  102.7 4.5 %fusion.6 = bf16[80,2048]{1,0:T(8,128)(2,1)} fusion(bf16[1,704,2048]{2,1,0:T(8,128)(2,1)S(1)} %copy-done, bf16[80,2048]{1,0:T(8,128)(2,1)} %reshape.74, bf16[1,2048,704]{1,2,0:T(8,128)(2,1)} %param.30, f32[80,704]{1,0:T(8,128)} %fusion.4), kind=kOutput, calls=%fused_computation.6 | convolution fusion | flops 461875200 | bytes 6647808 | tf_op jit(solution)/shard_map/dot_general | solution.py:31
  107.3 0.2 fusion.64
  107.6 2.5 %psum.29 = bf16[256]{0:T(256)(128)(2,1)S(1)} all-reduce(bf16[256]{0:T(256)(128)(2,1)S(1)} %convert_element_type.119), channel_id=1, replica_groups=mesh['ep'=16,'tp'=2] {'tp'}, use_global_device_ids=true, to_apply=%region_11.12 | all-reduce | flops 256 | bytes 1024 | tf_op jit(solution)/shard_map/psum | solution.py:114
  110.1 2.4 %fusion.39 = f32[256,1024]{1,0:T(8,128)} fusion(bf16[176,1024]{1,0:T(8,128)(2,1)} %param.28, bf16[256,176]{0,1:T(8,128)(2,1)} %get-tuple-element.4, bf16[256,176]{0,1:T(8,128)(2,1)} %get-tuple-element.5, f32[256]{0:T(256)S(1)} %add_divide_fusion), kind=kOutput, calls=%fused_computation.47 | convolution fusion | flops 92680192 | bytes 1590272 | tf_op jit(solution)/shard_map/dot_general | solution.py:136
  112.5 7.0 %reduce-scatter.6.cloned.1.call-done = bf16[80,1024]{1,0:T(8,128)(2,1)} async-done(((bf16[80,2048]{1,0:T(8,128)(2,1)}), bf16[80,1024]{1,0:T(8,128)(2,1)}) %reduce-scatter.6.cloned.1.call-update) | async-done | bytes 163856 | tf_op jit(solution)/shard_map/reduce_scatter | solution.py:38
  119.6 1.0 convert_element_type.118
  120.6 18.1 %all_to_all.10 = bf16[16,5,1024]{2,1,0:T(8,128)(2,1)S(1)} all-to-all(bf16[16,5,1024]{2,1,0:T(8,128)(2,1)S(1)} %convert_element_type.118), channel_id=1, replica_groups=mesh['ep'=16,'tp'=2] {'ep'}, dimensions={0} | all-to-all | bytes 327680 | tf_op jit(solution)/shard_map/all_to_all | solution.py:129
  138.8 63.0 %reduce-scatter.8.cloned.1.call-done = f32[16,1024]{1,0:T(8,128)} async-done(((f32[256,1024]{1,0:T(8,128)}), f32[16,1024]{1,0:T(8,128)}) %reduce-scatter.8.cloned.1.call-update) | async-done | bytes 65552 | tf_op jit(solution)/shard_map/reduce_scatter | solution.py:137
  201.7 1.8 fusion.17
  (46 shorter events, 1.0 us)
Async XLA Ops:
  7.2 95.6 %copy-start = (bf16[1,704,2048]{2,1,0:T(8,128)(2,1)S(1)}, bf16[1,704,2048]{2,1,0:T(8,128)(2,1)}, u32[]{:S(2)}) copy-start(bf16[1,704,2048]{2,1,0:T(8,128)(2,1)} %param.31) | copy-start | bytes 8650756
  7.2 24.4 %reduce-scatter.4.cloned.1.call-start = ((), (), s32[]{:S(2)}) async-start(), calls=%async_computation.5 | async-start | bytes 98304 | tf_op jit(solution)/shard_map/reduce_scatter | solution.py:99
  14.4 6.9 %copy-start.5 = (bf16[1024]{0:T(1024)(128)(2,1)S(1)}, bf16[1024]{0:T(1024)(128)(2,1)}, u32[]{:S(2)}) copy-start(bf16[1024]{0:T(1024)(128)(2,1)} %param.25) | copy-start | bytes 6148
  14.4 7.0 %copy-start.7 = (bf16[16,2]{0,1:T(2,128)(2,1)S(1)}, bf16[16,2]{0,1:T(2,128)(2,1)}, u32[]{:S(2)}) copy-start(bf16[16,2]{0,1:T(2,128)(2,1)} %param.33) | copy-start | bytes 196
  14.4 7.0 %copy-start.6 = (s32[16,2]{0,1:T(2,128)S(1)}, s32[16,2]{0,1:T(2,128)}, u32[]{:S(2)}) copy-start(s32[16,2]{0,1:T(2,128)} %param.32) | copy-start | bytes 388
  14.4 17.2 %copy-start.2 = (bf16[16,1024]{1,0:T(8,128)(2,1)S(1)}, bf16[16,1024]{1,0:T(8,128)(2,1)}, u32[]{:S(2)}) copy-start(bf16[16,1024]{1,0:T(8,128)(2,1)} %param.17) | copy-start | bytes 98308
  14.4 20.5 %copy-start.4 = (f32[1024]{0:T(1024)S(1)}, f32[1024]{0:T(1024)}, u32[]{:S(2)}) copy-start(f32[1024]{0:T(1024)} %param.24) | copy-start | bytes 12292
  16.4 1.3 copy-start.1
  80.7 12.7 %all-to-all-start = ((bf16[16,5,1024]{2,1,0:T(8,128)(2,1)}), bf16[16,5,1024]{2,1,0:T(8,128)(2,1)}, u32[]{:S(2)}, u32[]{:S(2)}) async-start(bf16[16,5,1024]{2,1,0:T(8,128)(2,1)} %bitcast.63), calls=%async_computation.1 | async-start | bytes 524288 | tf_op jit(solution)/shard_map/all_to_all | solution.py:127
  84.9 25.2 %all-reduce.3.cloned.1.call-start = ((), (), s32[]{:S(2)}) async-start(), calls=%async_computation.8 | async-start | bytes 360448 | tf_op jit(solution)/shard_map/psum | solution.py:113
  88.9 30.7 %reduce-scatter.6.cloned.1.call-start = ((), (), s32[]{:S(2)}) async-start(), calls=%async_computation.6 | async-start | bytes 491520 | tf_op jit(solution)/shard_map/reduce_scatter | solution.py:38
  107.2 94.5 %copy-start.3 = (bf16[16,1024]{1,0:T(8,128)(2,1)S(1)}, bf16[16,1024]{1,0:T(8,128)(2,1)}, u32[]{:S(2)}) copy-start(bf16[16,1024]{1,0:T(8,128)(2,1)} %reduce-scatter.4.cloned.1.call-done) | copy-start | bytes 98308
  107.3 94.4 %reduce-scatter.8.cloned.1.call-start = ((), (), s32[]{:S(2)}) async-start(), calls=%async_computation.7 | async-start | bytes 1114112 | tf_op jit(solution)/shard_map/reduce_scatter | solution.py:137
Sparse Core Ops, SparseCore 0:
  21.4 10.1 reduce-scatter.3
  89.0 19.2 all-reduce.2
  110.6 8.9 reduce-scatter.5
  121.7 79.9 reduce-scatter.7
where the time goes:
time: 211 us; the launch traced here: 210 us
  waiting for transfers between devices  84.5 us (40%)
  blocking collectives  73.3 us (35%)
  matrix products  24.3 us (12%)
  between operations  14 us (7%)
  local copies, waits for them, and re-layouts  5.22 us (2%)
  starting transfers between devices  4.35 us (2%)
  other arithmetic  4.33 us (2%)
    reduce_scatter x1, waiting for transfers between devices, body(): combined = lax.psum_scatter(value, 'ep', scatter_dimension=0, tiled=True)  63 us
    all_gather x1, blocking collectives, body(): all_rows = lax.all_gather(normed2, 'ep', axis=0, tiled=True)  44 us
    all_to_all x1, blocking collectives, body(): lax.all_to_all(served.astype(jnp.bfloat16), 'ep', split_axis=0, concat_ax...  18.1 us
    reduce_scatter x1, waiting for transfers between devices, body(): lax.psum_scatter(mix_part.astype(jnp.bfloat16), 'tp', scatter_dimension=1...  10 us
    reduce_scatter x1, waiting for transfers between devices, expert_apply(): lax.psum_scatter(partial_value.astype(jnp.bfloat16), 'tp', scatter_dimens...  7.02 us
    dot_general x1, matrix products, expert_math(): return jnp.dot(hidden, weights[2], preferred_element_type=jnp.float32)  4.51 us
    all_to_all x1, waiting for transfers between devices, body(): lax.all_to_all(outgoing, 'ep', split_axis=0, concat_axis=0, tiled=True)  4.47 us
  transfers between devices with their start and end apart: 5, of which 4 were waited for; matrix products, arithmetic and copies ran while one was open for 8% of the time, Pallas kernels for 0%

commit v1 on v0

v1 whole, which is shorter than its diff:
```python
import functools

import jax
import jax.numpy as jnp
from jax import lax
from jax.experimental import pallas as pl
from jax.experimental.pallas import tpu as pltpu
from jax.sharding import PartitionSpec as P

EXPERTS = 8
epsilon = 1e-06
MESH = pl.DeviceIdType.MESH
F32 = jnp.float32
BF16 = jnp.bfloat16


def dot(a, b):
    return jnp.dot(a, b, preferred_element_type=F32)


def silu(v):
    return v / (1.0 + jnp.exp(-v))


def kernel(
    A,
    B,
    tokens,
    norm_mix,
    routes,
    route_w,
    extra,
    state,
    w_query,
    w_key,
    w_value,
    w_out,
    dense_gate,
    dense_up,
    dense_down,
    exp_gate,
    exp_up,
    exp_down,
    mixed,
    new_state,
    tok_p,
    ext_p,
    wq,
    wk,
    wv,
    wo_o,
    wo_p,
    dg,
    du,
    dd,
    eg,
    eu,
    ed,
    st,
    ns,
    ho_o,
    ho_p,
    aux,
    xo,
    xp,
    y0,
    yx_s,
    yx_r,
    ys,
    rsx,
    zs,
    rsz,
    lsem,
    psem_s,
    psem_r,
    axz_s,
    axz_r,
    axx_s,
    axx_r,
    gz_s,
    gz_r,
    gx_s,
    gx_r,
    gp_s,
    gp_r,
    yx_ss,
    yx_rs,
    rx_s,
    rx_r,
    rz_s,
    rz_r,
):
    R, H = tokens.shape
    D = 2 * H
    heads, hs = state.shape[1], state.shape[2]
    HW = heads * hs
    n = A * B
    me = lax.axis_index("ep")
    tp = lax.axis_index("tp")
    z, xy = me // B, me % B
    other = 1 - tp
    expert = me // (n // EXPERTS)
    partner = {"ep": me, "tp": other}
    xpeer = [{"ep": z * B + (xy + j) % B, "tp": tp} for j in range(B)]
    zpeer = [{"ep": ((z + i) % A) * B + xy, "tp": tp} for i in range(A)]

    own_at = pl.multiple_of(tp * H, H)
    oth_at = pl.multiple_of(other * H, H)
    own, oth = pl.ds(own_at, H), pl.ds(oth_at, H)

    sent = []

    def remote(src, dst, s, r, dev):
        copy = pltpu.make_async_remote_copy(
            src_ref=src, dst_ref=dst, send_sem=s, recv_sem=r, device_id=dev, device_id_type=MESH
        )
        copy.start()
        sent.append(copy)
        return copy

    local = {}

    def load(name, k, src, dst):
        copy = pltpu.make_async_copy(src, dst, lsem.at[k])
        copy.start()
        local[name] = copy

    barrier = pltpu.get_barrier_semaphore()
    for dev in [partner] + xpeer[1:] + zpeer[1:]:
        pl.semaphore_signal(barrier, inc=1, device_id=dev, device_id_type=MESH)

    for t, (src, dst) in enumerate(((w_query, wq), (w_key, wk), (w_value, wv))):
        load(f"p{t}o", 2 * t, src.at[own, :], dst.at[0])
        load(f"p{t}p", 2 * t + 1, src.at[oth, :], dst.at[1])
    load("st", 6, state, st)
    load("wo0", 7, w_out.at[:, own], wo_o.at[0])
    load("wo1", 8, w_out.at[:, oth], wo_o.at[1])
    load("dg", 9, dense_gate, dg.at[0])
    load("du", 10, dense_up, du.at[0])
    load("dd", 11, dense_down, dd)
    load("eg0", 12, exp_gate.at[0, own, :], eg.at[0])
    load("eu0", 13, exp_up.at[0, own, :], eu.at[0])
    load("eg1", 14, exp_gate.at[0, oth, :], eg.at[1])
    load("eu1", 15, exp_up.at[0, oth, :], eu.at[1])
    load("ed1", 16, exp_down.at[0, :, oth], ed.at[1])
    load("ed0", 17, exp_down.at[0, :, own], ed.at[0])

    lane = lax.broadcasted_iota(jnp.int32, (R, 128), 1)
    wt = jnp.zeros((R, 128), F32)
    for t in range(routes.shape[1]):
        wt = wt + jnp.where(lane == routes[:, t : t + 1], route_w[:, t : t + 1].astype(F32), 0.0)
    aux[0, 0] = wt.astype(BF16)

    pl.semaphore_wait(barrier, 1 + (B - 1) + (A - 1))

    c_tok = remote(tokens, tok_p, psem_s.at[0], psem_r.at[0], partner)
    c_ext = remote(extra, ext_p, psem_s.at[1], psem_r.at[1], partner)
    c_wo0 = remote(w_out.at[:, oth], wo_p.at[0], psem_s.at[2], psem_r.at[2], partner)
    c_wo1 = remote(w_out.at[:, own], wo_p.at[1], psem_s.at[3], psem_r.at[3], partner)
    c_dg = remote(dense_gate, dg.at[1], psem_s.at[4], psem_r.at[4], partner)
    c_du = remote(dense_up, du.at[1], psem_s.at[5], psem_r.at[5], partner)
    c_axz = [None] + [
        remote(aux.at[0, 0], aux.at[0, A - i], axz_s.at[i], axz_r.at[A - i], zpeer[i])
        for i in range(1, A)
    ]

    tok_f = tokens[...].astype(F32)
    c_tok.wait_recv()
    tok_pf = tok_p[...].astype(F32)
    total = jnp.sum(tok_f * tok_f, axis=1, keepdims=True) + jnp.sum(
        tok_pf * tok_pf, axis=1, keepdims=True
    )
    scale = lax.rsqrt(total / D + epsilon)
    gain_o = norm_mix[:, own]
    gain_p = norm_mix[:, oth]
    nx_o = (tok_f * scale * gain_o).astype(BF16)
    nx_p = (tok_pf * scale * gain_p).astype(BF16)
    proj = []
    for t, w in enumerate((wq, wk, wv)):
        local[f"p{t}o"].wait()
        part = dot(nx_o, w[0])
        local[f"p{t}p"].wait()
        proj.append((part + dot(nx_p, w[1])).astype(BF16).astype(F32))
    q, k, v = proj
    k = k * hs ** (-0.5)
    pad = jnp.zeros((128 - R, HW), F32)
    q_t = jnp.concatenate([q, pad], axis=0).T
    k_t = jnp.concatenate([k, pad], axis=0).T
    head_id = tp * heads
    local["st"].wait()
    decays = []
    for h in range(heads):
        cols = slice(h * hs, (h + 1) * hs)
        idv = jnp.zeros((1, 128), F32) + (head_id + h).astype(F32)
        decay = 1.0 - jnp.exp2(-3.0 - 2.0 * idv)
        decays.append(decay)
        rows = []
        for s in range(R):
            rows.append(jnp.sum(st[s, h] * q_t[cols, s : s + 1], axis=0, keepdims=True))
        qs = jnp.concatenate(rows, axis=0)
        qk = jnp.sum(q[:, cols] * k[:, cols], axis=1, keepdims=True)
        read = decay * qs + qk * v[:, cols]
        centre = jnp.mean(read, axis=1, keepdims=True)
        dev = read - centre
        spread = jnp.mean(dev * dev, axis=1, keepdims=True)
        ho_o[:, cols] = (dev * lax.rsqrt(spread + epsilon)).astype(BF16)
    c_ho = remote(ho_o, ho_p, psem_s.at[6], psem_r.at[6], partner)
    ho = ho_o[...]
    local["wo0"].wait()
    local["wo1"].wait()
    a_o = dot(ho, wo_o[0]).astype(BF16).astype(F32)
    a_p = dot(ho, wo_o[1]).astype(BF16).astype(F32)
    c_wo0.wait_recv()
    c_wo1.wait_recv()
    c_ho.wait_recv()
    hp = ho_p[...]
    a_o = a_o + dot(hp, wo_p[0]).astype(BF16).astype(F32)
    a_p = a_p + dot(hp, wo_p[1]).astype(BF16).astype(F32)
    after = (tok_f + a_o).astype(BF16).astype(F32)
    after_p = (tok_pf + a_p).astype(BF16).astype(F32)
    squares = jnp.sum(after * after, axis=1, keepdims=True) + jnp.sum(
        after_p * after_p, axis=1, keepdims=True
    )
    xo[0, 0] = (after * lax.rsqrt(squares / D + epsilon) * extra[0:1, :]).astype(BF16)

    c_gz = [None] * A
    c_gx = {}
    c_gp = {}
    for i in range(1, A):
        c_gz[i] = remote(xo.at[0, 0], xo.at[0, A - i], gz_s.at[i], gz_r.at[A - i], zpeer[i])

    def spread_block(i):
        for j in range(1, B):
            c_gx[j, i] = remote(
                xo.at[0, i],
                xo.at[B - j, i],
                gx_s.at[j, i],
                gx_r.at[B - j, i],
                xpeer[j],
            )

    def to_partner(j, i):
        c_gp[j, i] = remote(
            xo.at[j, i], xp.at[j, i], gp_s.at[j, i], gp_r.at[j, i], partner
        )

    spread_block(0)
    to_partner(0, 0)
    for i in range(1, A):
        c_axz[A - i].wait_recv()
    c_axx = [None] + [
        remote(aux.at[0], aux.at[B - j], axx_s.at[j], axx_r.at[B - j], xpeer[j])
        for j in range(1, B)
    ]
    order = sorted(range(1, A), key=lambda i: min(i, A - i))
    for i in order:
        c_gz[A - i].wait_recv()
        spread_block(i)
        to_partner(0, i)

    for h in range(heads):
        cols = slice(h * hs, (h + 1) * hs)
        for s in range(R):
            ns[s, h] = decays[h] * st[s, h] + k_t[cols, s : s + 1] * v[s : s + 1, cols]
    c_ns = pltpu.make_async_copy(ns, new_state, lsem.at[18])
    c_ns.start()

    c_ext.wait_recv()
    for name in ("dg", "du", "dd", "eg0", "eu0", "eg1", "eu1", "ed1", "ed0"):
        local[name].wait()
    c_dg.wait_recv()
    c_du.wait_recv()

    AR = A * R

    def ffn(j0, nj, slot):
        rows = nj * AR
        x_o = xo[j0 : j0 + nj].reshape(rows, H)
        gate = dot(x_o, eg[0])
        up = dot(x_o, eu[0])
        d_gate = dot(x_o, dg[0])
        d_up = dot(x_o, du[0])
        logit = jnp.sum(x_o.astype(F32) * extra[1:2, :], axis=1, keepdims=True)
        for j in range(j0, j0 + nj):
            for i in range(A):
                c_gp[j, i].wait_recv()
        x_p = xp[j0 : j0 + nj].reshape(rows, H)
        gate = gate + dot(x_p, eg[1])
        up = up + dot(x_p, eu[1])
        d_gate = d_gate + dot(x_p, dg[1])
        d_up = d_up + dot(x_p, du[1])
        logit = logit + jnp.sum(x_p.astype(F32) * ext_p[1:2, :], axis=1, keepdims=True)
        lanes = lax.broadcasted_iota(jnp.int32, (rows, 128), 1)
        table = aux[j0 : j0 + nj].reshape(rows, 128).astype(F32)
        weight = jnp.sum(jnp.where(lanes == expert, table, 0.0), axis=1, keepdims=True)
        hidden = (silu(gate) * up).astype(BF16)
        d_hidden = (1.0 / (1.0 + jnp.exp(-logit)) * silu(d_gate) * d_up).astype(BF16)
        yx_s[j0 : j0 + nj] = (weight * dot(hidden, ed[1])).astype(BF16).reshape(nj, A, R, H)
        c_yx = remote(
            yx_s.at[pl.ds(j0, nj)],
            yx_r.at[pl.ds(j0, nj)],
            yx_ss.at[slot],
            yx_rs.at[slot],
            partner,
        )
        y = weight * dot(hidden, ed[0]) + dot(d_hidden, dd[...])
        c_yx.wait_recv()
        return y.reshape(nj, A, R, H) + yx_r[j0 : j0 + nj].astype(F32)

    y0[...] = ffn(0, 1, 0)[0]

    for i in [0] + order:
        for j in range(1, B):
            c_gx[B - j, i].wait_recv()
            to_partner(j, i)
    for j in range(1, B):
        c_axx[B - j].wait_recv()
    group = max(g for g in range(1, B) if (B - 1) % g == 0 and (g * AR <= 256 or g == 1))
    c_rx = [None] * B
    for slot, j0 in enumerate(range(1, B, group)):
        y = ffn(j0, group, slot + 1)
        ys[j0 : j0 + group] = y.astype(BF16)
        for j in range(j0, j0 + group):
            c_rx[j] = remote(ys.at[j], rsx.at[B - j], rx_s.at[j], rx_r.at[B - j], xpeer[j])

    total = y0[...]
    for j in range(1, B):
        c_rx[B - j].wait_recv()
        total = total + rsx[j].astype(F32)
    zs[...] = total.astype(BF16)
    c_rz = [None] + [
        remote(zs.at[i], rsz.at[A - i], rz_s.at[i], rz_r.at[A - i], zpeer[i])
        for i in range(1, A)
    ]
    result = after + total[0]
    for i in range(1, A):
        c_rz[A - i].wait_recv()
        result = result + rsz[i].astype(F32)
    mixed[...] = result.astype(BF16)
    for copy in sent:
        copy.wait_send()
    c_ns.wait()


def body(
    tokens,
    state,
    norm_mix,
    w_query,
    w_key,
    w_value,
    w_out,
    norm_ffn,
    gate_vector,
    dense_gate,
    dense_up,
    dense_down,
    exp_gate,
    exp_up,
    exp_down,
    routes,
    route_w,
):
    n = lax.axis_size("ep")
    A = 1
    while (2 * A) * (2 * A) <= n:
        A = 2 * A
    B = n // A
    R, H = tokens.shape
    heads, hs = state.shape[1], state.shape[2]
    HW = heads * hs
    FE = exp_gate.shape[2]
    FD = dense_gate.shape[1]
    extra = jnp.stack([norm_ffn, gate_vector.astype(F32)])
    vm = pl.BlockSpec(memory_space=pltpu.VMEM)
    hbm = pl.BlockSpec(memory_space=pl.ANY)
    V = pltpu.VMEM
    sem = lambda *shape: pltpu.SemaphoreType.DMA(shape)
    return pl.pallas_call(
        functools.partial(kernel, A, B),
        out_shape=(
            jax.ShapeDtypeStruct((R, H), BF16),
            jax.ShapeDtypeStruct(state.shape, F32),
        ),
        in_specs=[vm] * 5 + [hbm] * 11,
        out_specs=(vm, hbm),
        scratch_shapes=[
            V((R, H), BF16),
            V((2, H), F32),
            V((2, H, HW), BF16),
            V((2, H, HW), BF16),
            V((2, H, HW), BF16),
            V((2, HW, H), BF16),
            V((2, HW, H), BF16),
            V((2, H, FD), BF16),
            V((2, H, FD), BF16),
            V((FD, H), BF16),
            V((2, H, FE), BF16),
            V((2, H, FE), BF16),
            V((2, FE, H), BF16),
            V(state.shape, F32),
            V(state.shape, F32),
            V((R, HW), BF16),
            V((R, HW), BF16),
            V((B, A, R, 128), BF16),
            V((B, A, R, H), BF16),
            V((B, A, R, H), BF16),
            V((A, R, H), F32),
            V((B, A, R, H), BF16),
            V((B, A, R, H), BF16),
            V((B, A, R, H), BF16),
            V((B, A, R, H), BF16),
            V((A, R, H), BF16),
            V((A, R, H), BF16),
            sem(19),
            sem(7),
            sem(7),
            sem(A),
            sem(A),
            sem(B),
            sem(B),
            sem(A),
            sem(A),
            sem(B, A),
            sem(B, A),
            sem(B, A),
            sem(B, A),
            sem(B),
            sem(B),
            sem(B),
            sem(B),
            sem(A),
            sem(A),
        ],
        compiler_params=pltpu.CompilerParams(
            collective_id=0, has_side_effects=True, vmem_limit_bytes=67043328
        ),
        name="layer",
    )(
        tokens,
        norm_mix.reshape(1, -1),
        routes,
        route_w,
        extra,
        state,
        w_query,
        w_key,
        w_value,
        w_out,
        dense_gate,
        dense_up,
        dense_down,
        exp_gate,
        exp_up,
        exp_down,
    )


def solution(mesh):
    return jax.shard_map(
        body,
        mesh=mesh,
        in_specs=(
            P("ep", "tp"),
            P("ep", "tp", None, None),
            P(),
            P(None, "tp"),
            P(None, "tp"),
            P(None, "tp"),
            P("tp", None),
            P("tp"),
            P("tp"),
            P("tp", "ep"),
            P("tp", "ep"),
            P("ep", "tp"),
            P("ep", None, "tp"),
            P("ep", None, "tp"),
            P("ep", "tp", None),
            P("ep", None),
            P("ep", None),
        ),
        out_specs=(P("ep", "tp"), P("ep", "tp", None, None)),
        check_vma=False,
    )
```

time: 211 us -> 61.6 us (0.29)
  waiting for transfers between devices: 84.5 us -> 0 us
  blocking collectives: 73.3 us -> 0 us
  Pallas kernels: 0 us -> 39.7 us
  matrix products: 24.3 us -> 0 us
  local copies, waits for them, and re-layouts: 5.22 us -> 18.8 us
  between operations: 14 us -> 0.64 us
  starting transfers between devices: 4.35 us -> 0 us
  other arithmetic: 4.33 us -> 1.97 us
    reduce_scatter x3 -> x0, waiting for transfers between devices: 80 us -> none  [the longest x1 63 us: body(): combined = lax.psum_scatter(value, 'ep', scatter_dimension=0, tiled=True)]
    all_gather x3 -> x0, blocking collectives: 50.1 us -> none  [the longest x1 44 us: body(): all_rows = lax.all_gather(normed2, 'ep', axis=0, tiled=True)]
    pallas_call x0 -> x1, Pallas kernels: none -> 39.7 us  [body(): pl.pallas_call(functools.partial(kernel, A, B), out_shape=(jax.ShapeDtype...]
    dot_general x13 -> x0, matrix products: 24.3 us -> none  [the longest x1 4.51 us: expert_math(): return jnp.dot(hidden, weights[2], preferred_element_type=jnp.float32)]
    all_to_all x1 -> x0, blocking collectives: 18.1 us -> none  [body(): lax.all_to_all(served.astype(jnp.bfloat16), 'ep', split_axis=0, concat_ax...]
    unnamed x17 -> x10, local copies, waits for them, and re-layouts: 1.36 us -> 18.8 us
    psum x2 -> x0, blocking collectives: 4.97 us -> none  [the longest x1 2.51 us: body(): lax.psum(logit.astype(jnp.bfloat16), 'tp').astype(jnp.float32)]
    all_to_all x1 -> x0, waiting for transfers between devices: 4.47 us -> none  [body(): lax.all_to_all(outgoing, 'ep', split_axis=0, concat_axis=0, tiled=True)]
  transfers between devices with their start and end apart: 5 -> 0, of which waited for: 4 -> 0; matrix products, arithmetic and copies ran while one was open for 8% -> 0% of each run, Pallas kernels for 0% -> 0%
where the time goes in v1:
time: 61.6 us; the launch traced here: 61.1 us
  Pallas kernels  39.7 us (64%)
  local copies, waits for them, and re-layouts  18.8 us (31%)
  other arithmetic  1.97 us (3%)
  between operations  0.64 us (1%)
    pallas_call x1, Pallas kernels, body(): pl.pallas_call(functools.partial(kernel, A, B), out_shape=(jax.ShapeDtype...  39.7 us
    unnamed x10, local copies, waits for them, and re-layouts  18.8 us
    another operation x2, other arithmetic, body(): extra = jnp.stack([norm_ffn, gate_vector.astype(F32)])  1.97 us

profile of v1, /device:TPU:0, one launch (start us, length us, event | category | flops | bytes accessed | tf_op | source)
XLA Modules:
  0.0 61.1 jit_solution(7665546844379814286)
XLA Ops:
  0.6 0.7 %stack.16 = f32[1024]{0:T(1024)S(1)} convert(bf16[1024]{0:T(1024)(128)(2,1)} %param.25) | non-fusion elementwise | flops 1024 | bytes 6144 | tf_op jit(solution)/shard_map/stack | solution.py:374
  1.3 1.3 %pad_maximum_fusion.extra = f32[2,1024]{1,0:T(2,128)} fusion(f32[1,1024]{1,0:T(1,128)S(1)} %bitcast.3, f32[1,1024]{1,0:T(1,128)} %bitcast.5), kind=kLoop, calls=%fused_computation | loop fusion | flops 2048 | bytes 16384 | tf_op jit(solution)/shard_map/stack | solution.py:374
  2.6 1.3 %copy.20.route_w = bf16[16,2]{1,0:T(8,128)(2,1)} copy(bf16[16,2]{0,1:T(2,128)(2,1)} %param.33) | data formatting | bytes 128 | tf_op args[16]
  3.9 1.4 %copy.19.routes = s32[16,2]{1,0:T(8,128)} copy(s32[16,2]{0,1:T(2,128)} %param.32) | data formatting | bytes 256 | tf_op args[15]
  5.3 2.0 %copy.21.dense_gate = bf16[1024,176]{1,0:T(8,128)(2,1)} copy(bf16[1024,176]{0,1:T(8,128)(2,1)} %param.26) | data formatting | bytes 720896 | tf_op args[9]
  7.3 2.0 %copy.22.dense_up = bf16[1024,176]{1,0:T(8,128)(2,1)} copy(bf16[1024,176]{0,1:T(8,128)(2,1)} %param.27) | data formatting | bytes 720896 | tf_op args[10]
  9.3 0.0 copy-start
  9.3 4.7 %copy.23.exp_gate = bf16[1,2048,704]{2,1,0:T(8,128)(2,1)} copy(bf16[1,2048,704]{1,2,0:T(8,128)(2,1)} %param.29) | data formatting | bytes 5767168 | tf_op args[12]
  14.0 0.0 copy-done
  14.0 2.8 %copy.24.exp_up = bf16[1,2048,704]{2,1,0:T(8,128)(2,1)} copy(bf16[1,2048,704]{1,2,0:T(8,128)(2,1)S(1)} %copy-done) | data formatting | bytes 5767168 | tf_op args[13]
  16.8 39.7 %layer.1 = (bf16[16,1024]{1,0:T(8,128)(2,1)}, f32[16,2,128,128]{3,2,1,0:T(8,128)}) custom-call(bf16[16,1024]{1,0:T(8,128)(2,1)} %tokens.1, f32[1,2048]{1,0:T(1,128)} %bitcast.4, s32[16,2]{1,0:T(8,128)} %copy.19.routes, bf16[16,2]{1,0:T(8,128)(2,1)} %copy.20.route_w, f32[2,1024]{1,0:T(2,128)} %pad_maximum_fusion.extra, f32[16,2,128,128]{3,2,1,0:T(8,128)} %state.1, ...), custom_call_target="tpu_custom_call" | custom-call | tf_op jit(solution)/shard_map/layer/pallas_call | solution.py:379
  56.6 1.4 %copy.27 = bf16[16,1024]{1,0:T(8,128)(2,1)} copy(bf16[16,1024]{1,0:T(8,128)(2,1)} %get-tuple-element.4) | data formatting | bytes 65536
  58.0 3.1 %copy.28 = f32[16,2,128,128]{3,2,1,0:T(8,128)} copy(f32[16,2,128,128]{3,2,1,0:T(8,128)} %get-tuple-element.5) | data formatting | bytes 4194304
Async XLA Ops:
  9.3 4.7 %copy-start = (bf16[1,2048,704]{1,2,0:T(8,128)(2,1)S(1)}, bf16[1,2048,704]{1,2,0:T(8,128)(2,1)}, u32[]{:S(2)}) copy-start(bf16[1,2048,704]{1,2,0:T(8,128)(2,1)} %param.30) | copy-start | bytes 8650756

commit v2 on v1

--- a/solution.py
+++ b/solution.py
@@ -18,6 +18,10 @@
     return jnp.dot(a, b, preferred_element_type=F32)
 
 
+def dot_t(a, b):
+    return lax.dot_general(a, b, (((1,), (1,)), ((), ())), preferred_element_type=F32)
+
+
 def silu(v):
     return v / (1.0 + jnp.exp(-v))
 
@@ -25,11 +29,12 @@
 def kernel(
     A,
     B,
-    tokens,
-    norm_mix,
-    routes,
-    route_w,
-    extra,
+    tokens_h,
+    norm_mix_h,
+    routes_h,
+    route_w_h,
+    norm_ffn_h,
+    gate_vec_h,
     state,
     w_query,
     w_key,
@@ -42,9 +47,15 @@
     exp_up,
     exp_down,
     mixed,
-    new_state,
+    ns,
+    tokens,
+    norm_mix,
+    routes,
+    route_w,
+    norm_ffn,
+    gate_vec,
     tok_p,
-    ext_p,
+    gvec_p,
     wq,
     wk,
     wv,
@@ -57,7 +68,6 @@
     eu,
     ed,
     st,
-    ns,
     ho_o,
     ho_p,
     aux,
@@ -125,10 +135,20 @@
         copy.start()
         local[name] = copy
 
+    small = (
+        (tokens_h, tokens),
+        (norm_mix_h, norm_mix),
+        (routes_h, routes),
+        (route_w_h, route_w),
+        (norm_ffn_h, norm_ffn),
+        (gate_vec_h, gate_vec),
+    )
     barrier = pltpu.get_barrier_semaphore()
     for dev in [partner] + xpeer[1:] + zpeer[1:]:
         pl.semaphore_signal(barrier, inc=1, device_id=dev, device_id_type=MESH)
 
+    for t, (src, dst) in enumerate(small):
+        load(f"s{t}", 19 + t, src, dst)
     for t, (src, dst) in enumerate(((w_query, wq), (w_key, wk), (w_value, wv))):
         load(f"p{t}o", 2 * t, src.at[own, :], dst.at[0])
         load(f"p{t}p", 2 * t + 1, src.at[oth, :], dst.at[1])
@@ -138,23 +158,31 @@
     load("dg", 9, dense_gate, dg.at[0])
     load("du", 10, dense_up, du.at[0])
     load("dd", 11, dense_down, dd)
-    load("eg0", 12, exp_gate.at[0, own, :], eg.at[0])
-    load("eu0", 13, exp_up.at[0, own, :], eu.at[0])
-    load("eg1", 14, exp_gate.at[0, oth, :], eg.at[1])
-    load("eu1", 15, exp_up.at[0, oth, :], eu.at[1])
+    load("eg0", 12, exp_gate.at[:, own], eg.at[0])
+    load("eu0", 13, exp_up.at[:, own], eu.at[0])
+    load("eg1", 14, exp_gate.at[:, oth], eg.at[1])
+    load("eu1", 15, exp_up.at[:, oth], eu.at[1])
     load("ed1", 16, exp_down.at[0, :, oth], ed.at[1])
     load("ed0", 17, exp_down.at[0, :, own], ed.at[0])
 
-    lane = lax.broadcasted_iota(jnp.int32, (R, 128), 1)
-    wt = jnp.zeros((R, 128), F32)
-    for t in range(routes.shape[1]):
-        wt = wt + jnp.where(lane == routes[:, t : t + 1], route_w[:, t : t + 1].astype(F32), 0.0)
-    aux[0, 0] = wt.astype(BF16)
-
+    for t in (2, 3):
+        local[f"s{t}"].wait()
+    row_id = lax.broadcasted_iota(jnp.int32, (EXPERTS, R), 0)
+    wt = jnp.zeros((EXPERTS, R), F32)
+    named = routes[...]
+    gains = route_w[...].astype(F32)
+    for t in range(routes.shape[0]):
+        wt = wt + jnp.where(row_id == named[t : t + 1, :], gains[t : t + 1, :], 0.0)
+    wt = jnp.concatenate([wt, jnp.zeros((EXPERTS, 128 - R), F32)], axis=1)
+    wt = jnp.concatenate([wt, jnp.zeros((128 - EXPERTS, 128), F32)], axis=0)
+    aux[0, 0] = wt.T[:R].astype(BF16)
+
+    for t in (0, 1, 4, 5):
+        local[f"s{t}"].wait()
     pl.semaphore_wait(barrier, 1 + (B - 1) + (A - 1))
 
     c_tok = remote(tokens, tok_p, psem_s.at[0], psem_r.at[0], partner)
-    c_ext = remote(extra, ext_p, psem_s.at[1], psem_r.at[1], partner)
+    c_ext = remote(gate_vec, gvec_p, psem_s.at[1], psem_r.at[1], partner)
     c_wo0 = remote(w_out.at[:, oth], wo_p.at[0], psem_s.at[2], psem_r.at[2], partner)
     c_wo1 = remote(w_out.at[:, own], wo_p.at[1], psem_s.at[3], psem_r.at[3], partner)
     c_dg = remote(dense_gate, dg.at[1], psem_s.at[4], psem_r.at[4], partner)
@@ -221,7 +249,7 @@
     squares = jnp.sum(after * after, axis=1, keepdims=True) + jnp.sum(
         after_p * after_p, axis=1, keepdims=True
     )
-    xo[0, 0] = (after * lax.rsqrt(squares / D + epsilon) * extra[0:1, :]).astype(BF16)
+    xo[0, 0] = (after * lax.rsqrt(squares / D + epsilon) * norm_ffn[...]).astype(BF16)
 
     c_gz = [None] * A
     c_gx = {}
@@ -262,8 +290,6 @@
         cols = slice(h * hs, (h + 1) * hs)
         for s in range(R):
             ns[s, h] = decays[h] * st[s, h] + k_t[cols, s : s + 1] * v[s : s + 1, cols]
-    c_ns = pltpu.make_async_copy(ns, new_state, lsem.at[18])
-    c_ns.start()
 
     c_ext.wait_recv()
     for name in ("dg", "du", "dd", "eg0", "eu0", "eg1", "eu1", "ed1", "ed0"):
@@ -273,23 +299,30 @@
 
     AR = A * R
 
+    def gate_row(ref):
+        part = ref[...].astype(F32)
+        return jnp.concatenate([part[r : r + 1] for r in range(H // 128)], axis=1)
+
+    gvec_o = gate_row(gate_vec)
+    gvec_q = gate_row(gvec_p)
+
     def ffn(j0, nj, slot):
         rows = nj * AR
         x_o = xo[j0 : j0 + nj].reshape(rows, H)
-        gate = dot(x_o, eg[0])
-        up = dot(x_o, eu[0])
-        d_gate = dot(x_o, dg[0])
-        d_up = dot(x_o, du[0])
-        logit = jnp.sum(x_o.astype(F32) * extra[1:2, :], axis=1, keepdims=True)
+        gate = dot_t(x_o, eg[0])
+        up = dot_t(x_o, eu[0])
+        d_gate = dot_t(x_o, dg[0])
+        d_up = dot_t(x_o, du[0])
+        logit = jnp.sum(x_o.astype(F32) * gvec_o, axis=1, keepdims=True)
         for j in range(j0, j0 + nj):
             for i in range(A):
                 c_gp[j, i].wait_recv()
         x_p = xp[j0 : j0 + nj].reshape(rows, H)
-        gate = gate + dot(x_p, eg[1])
-        up = up + dot(x_p, eu[1])
-        d_gate = d_gate + dot(x_p, dg[1])
-        d_up = d_up + dot(x_p, du[1])
-        logit = logit + jnp.sum(x_p.astype(F32) * ext_p[1:2, :], axis=1, keepdims=True)
+        gate = gate + dot_t(x_p, eg[1])
+        up = up + dot_t(x_p, eu[1])
+        d_gate = d_gate + dot_t(x_p, dg[1])
+        d_up = d_up + dot_t(x_p, du[1])
+        logit = logit + jnp.sum(x_p.astype(F32) * gvec_q, axis=1, keepdims=True)
         lanes = lax.broadcasted_iota(jnp.int32, (rows, 128), 1)
         table = aux[j0 : j0 + nj].reshape(rows, 128).astype(F32)
         weight = jnp.sum(jnp.where(lanes == expert, table, 0.0), axis=1, keepdims=True)
@@ -339,7 +372,15 @@
     mixed[...] = result.astype(BF16)
     for copy in sent:
         copy.wait_send()
-    c_ns.wait()
+
+
+def store(a_in, b_in, a_out, b_out, sems):
+    first = pltpu.make_async_copy(b_in, b_out, sems.at[0])
+    second = pltpu.make_async_copy(a_in, a_out, sems.at[1])
+    first.start()
+    second.start()
+    first.wait()
+    second.wait()
 
 
 def body(
@@ -371,34 +412,55 @@
     HW = heads * hs
     FE = exp_gate.shape[2]
     FD = dense_gate.shape[1]
-    extra = jnp.stack([norm_ffn, gate_vector.astype(F32)])
     vm = pl.BlockSpec(memory_space=pltpu.VMEM)
-    hbm = pl.BlockSpec(memory_space=pl.ANY)
+    hbm = pl.BlockSpec(memory_space=pltpu.HBM)
     V = pltpu.VMEM
     sem = lambda *shape: pltpu.SemaphoreType.DMA(shape)
-    return pl.pallas_call(
+    operands = (
+        tokens,
+        norm_mix.reshape(1, -1),
+        routes.T,
+        route_w.T,
+        norm_ffn.reshape(1, -1),
+        gate_vector.reshape(-1, 128),
+        state,
+        w_query,
+        w_key,
+        w_value,
+        w_out,
+        dense_gate.T,
+        dense_up.T,
+        dense_down,
+        exp_gate[0].T,
+        exp_up[0].T,
+        exp_down,
+    )
+    held = [pltpu.with_memory_space_constraint(x, pltpu.HBM) for x in operands]
+    mixed, new_state = pl.pallas_call(
         functools.partial(kernel, A, B),
-        out_shape=(
-            jax.ShapeDtypeStruct((R, H), BF16),
-            jax.ShapeDtypeStruct(state.shape, F32),
-        ),
-        in_specs=[vm] * 5 + [hbm] * 11,
-        out_specs=(vm, hbm),
+        out_shape=(pltpu.VMEM((R, H), BF16), pltpu.VMEM(state.shape, F32)),
+        in_specs=[hbm] * 17,
+        out_specs=(vm, vm),
         scratch_shapes=[
             V((R, H), BF16),
-            V((2, H), F32),
+            V((1, 2 * H), F32),
+            V((routes.shape[1], R), jnp.int32),
+            V((routes.shape[1], R), BF16),
+            V((1, H), F32),
+            V((H // 128, 128), BF16),
+            V((R, H), BF16),
+            V((H // 128, 128), BF16),
             V((2, H, HW), BF16),
             V((2, H, HW), BF16),
             V((2, H, HW), BF16),
             V((2, HW, H), BF16),
             V((2, HW, H), BF16),
-            V((2, H, FD), BF16),
-            V((2, H, FD), BF16),
+            V((2, FD, H), BF16),
+            V((2, FD, H), BF16),
             V((FD, H), BF16),
-            V((2, H, FE), BF16),
-            V((2, H, FE), BF16),
             V((2, FE, H), BF16),
-            V(state.shape, F32),
+            V((2, FE, H), BF16),
+            V((2, FE, H), BF16),
             V(state.shape, F32),
             V((R, HW), BF16),
             V((R, HW), BF16),
@@ -412,7 +474,7 @@
             V((B, A, R, H), BF16),
             V((A, R, H), BF16),
             V((A, R, H), BF16),
-            sem(19),
+            sem(25),
             sem(7),
             sem(7),
             sem(A),
@@ -433,26 +495,25 @@
             sem(A),
         ],
         compiler_params=pltpu.CompilerParams(
-            collective_id=0, has_side_effects=True, vmem_limit_bytes=67043328
+            collective_id=0, has_side_effects=True, vmem_limit_bytes=50 * 1024 * 1024
         ),
         name="layer",
     )(
-        tokens,
-        norm_mix.reshape(1, -1),
-        routes,
-        route_w,
-        extra,
-        state,
-        w_query,
-        w_key,
-        w_value,
-        w_out,
-        dense_gate,
-        dense_up,
-        dense_down,
-        exp_gate,
-        exp_up,
-        exp_down,
+        *held
+    )
+    return pl.pallas_call(
+        store,
+        out_shape=(
+            jax.ShapeDtypeStruct((R, H), BF16),
+            jax.ShapeDtypeStruct(state.shape, F32),
+        ),
+        in_specs=[vm, vm],
+        out_specs=(hbm, hbm),
+        scratch_shapes=[sem(2)],
+        name="store",
+    )(
+        pltpu.with_memory_space_constraint(mixed, pltpu.VMEM),
+        pltpu.with_memory_space_constraint(new_state, pltpu.VMEM),
     )
 
 

time: 61.6 us -> 40.3 us (0.65)
  local copies, waits for them, and re-layouts: 18.8 us -> 0 us
  other arithmetic: 1.97 us -> 0 us
    unnamed x10 -> x0, local copies, waits for them, and re-layouts: 18.8 us -> none
    another operation x2 -> x0, other arithmetic: 1.97 us -> none  [body(): extra = jnp.stack([norm_ffn, gate_vector.astype(F32)])]
    pallas_call x1 -> x2, Pallas kernels: 39.7 us -> 39.5 us  [the longest x1 38.1 us: body(): pl.pallas_call(functools.partial(kernel, A, B), out_shape=(pltpu.VMEM((R,...]
where the time goes in v2:
time: 40.3 us; the launch traced here: 40.1 us
  Pallas kernels  39.5 us (98%)
  between operations  0.65 us (2%)
    pallas_call x1, Pallas kernels, body(): pl.pallas_call(functools.partial(kernel, A, B), out_shape=(pltpu.VMEM((R,...  38.1 us
    pallas_call x1, Pallas kernels, body(): pl.pallas_call(store, out_shape=(jax.ShapeDtypeStruct((R, H), BF16), jax....  1.34 us

profile of v2, /device:TPU:0, one launch (start us, length us, event | category | flops | bytes accessed | tf_op | source)
XLA Modules:
  0.0 40.1 jit_solution(10429639955209649007)
XLA Ops:
  0.6 38.1 %layer.1 = (bf16[16,1024]{1,0:T(8,128)(2,1)S(1)}, f32[16,2,128,128]{3,2,1,0:T(8,128)S(1)}) custom-call(bf16[16,1024]{1,0:T(8,128)(2,1)} %tokens_h.1, f32[1,2048]{1,0:T(1,128)} %bitcast.17, s32[2,16]{1,0:T(2,128)} %bitcast.20, bf16[2,16]{1,0:T(2,128)(2,1)} %bitcast.21, f32[1,1024]{1,0:T(1,128)} %bitcast.18, bf16[8,128]{1,0:T(8,128)(2,1)} %bitcast.19, ...), custom_call_target="tpu_custom_call" | custom-call | tf_op jit(solution)/shard_map/layer/pallas_call | solution.py:439
  38.8 1.3 %store.1 = (bf16[16,1024]{1,0:T(8,128)(2,1)}, f32[16,2,128,128]{3,2,1,0:T(8,128)}) custom-call(bf16[16,1024]{1,0:T(8,128)(2,1)S(1)} %get-tuple-element.4.a_in, f32[16,2,128,128]{3,2,1,0:T(8,128)S(1)} %get-tuple-element.5.b_in), custom_call_target="tpu_custom_call" | custom-call | tf_op jit(solution)/shard_map/store/pallas_call | solution.py:504

commit v3 on v2

--- a/solution.py
+++ b/solution.py
@@ -8,6 +8,7 @@
 from jax.sharding import PartitionSpec as P
 
 EXPERTS = 8
+ROWS = 256
 epsilon = 1e-06
 MESH = pl.DeviceIdType.MESH
 F32 = jnp.float32
@@ -155,16 +156,6 @@
     load("st", 6, state, st)
     load("wo0", 7, w_out.at[:, own], wo_o.at[0])
     load("wo1", 8, w_out.at[:, oth], wo_o.at[1])
-    load("dg", 9, dense_gate, dg.at[0])
-    load("du", 10, dense_up, du.at[0])
-    load("dd", 11, dense_down, dd)
-    load("eg0", 12, exp_gate.at[:, own], eg.at[0])
-    load("eu0", 13, exp_up.at[:, own], eu.at[0])
-    load("eg1", 14, exp_gate.at[:, oth], eg.at[1])
-    load("eu1", 15, exp_up.at[:, oth], eu.at[1])
-    load("ed1", 16, exp_down.at[0, :, oth], ed.at[1])
-    load("ed0", 17, exp_down.at[0, :, own], ed.at[0])
-
     for t in (2, 3):
         local[f"s{t}"].wait()
     row_id = lax.broadcasted_iota(jnp.int32, (EXPERTS, R), 0)
@@ -187,8 +178,17 @@
     c_wo1 = remote(w_out.at[:, own], wo_p.at[1], psem_s.at[3], psem_r.at[3], partner)
     c_dg = remote(dense_gate, dg.at[1], psem_s.at[4], psem_r.at[4], partner)
     c_du = remote(dense_up, du.at[1], psem_s.at[5], psem_r.at[5], partner)
+    load("dg", 9, dense_gate, dg.at[0])
+    load("du", 10, dense_up, du.at[0])
+    load("dd", 11, dense_down, dd)
+    load("eg0", 12, exp_gate.at[:, own], eg.at[0])
+    load("eu0", 13, exp_up.at[:, own], eu.at[0])
+    load("eg1", 14, exp_gate.at[:, oth], eg.at[1])
+    load("eu1", 15, exp_up.at[:, oth], eu.at[1])
+    load("ed1", 16, exp_down.at[0, :, oth], ed.at[1])
+    load("ed0", 17, exp_down.at[0, :, own], ed.at[0])
     c_axz = [None] + [
-        remote(aux.at[0, 0], aux.at[0, A - i], axz_s.at[i], axz_r.at[A - i], zpeer[i])
+        remote(aux.at[0, 0], aux.at[A - i, 0], axz_s.at[i], axz_r.at[A - i], zpeer[i])
         for i in range(1, A)
     ]
 
@@ -255,49 +255,46 @@
     c_gx = {}
     c_gp = {}
     for i in range(1, A):
-        c_gz[i] = remote(xo.at[0, 0], xo.at[0, A - i], gz_s.at[i], gz_r.at[A - i], zpeer[i])
+        c_gz[i] = remote(xo.at[0, 0], xo.at[A - i, 0], gz_s.at[i], gz_r.at[A - i], zpeer[i])
 
     def spread_block(i):
         for j in range(1, B):
-            c_gx[j, i] = remote(
-                xo.at[0, i],
-                xo.at[B - j, i],
-                gx_s.at[j, i],
-                gx_r.at[B - j, i],
-                xpeer[j],
+            c_gx[i, j] = remote(
+                xo.at[i, 0], xo.at[i, B - j], gx_s.at[i, j], gx_r.at[i, B - j], xpeer[j]
             )
 
-    def to_partner(j, i):
-        c_gp[j, i] = remote(
-            xo.at[j, i], xp.at[j, i], gp_s.at[j, i], gp_r.at[j, i], partner
-        )
+    def to_partner(i, j):
+        c_gp[i, j] = remote(xo.at[i, j], xp.at[i, j], gp_s.at[i, j], gp_r.at[i, j], partner)
 
     spread_block(0)
     to_partner(0, 0)
-    for i in range(1, A):
-        c_axz[A - i].wait_recv()
-    c_axx = [None] + [
-        remote(aux.at[0], aux.at[B - j], axx_s.at[j], axx_r.at[B - j], xpeer[j])
-        for j in range(1, B)
-    ]
-    order = sorted(range(1, A), key=lambda i: min(i, A - i))
-    for i in order:
-        c_gz[A - i].wait_recv()
-        spread_block(i)
-        to_partner(0, i)
+    c_axx = {}
+    for i in range(A):
+        if i > 0:
+            c_axz[A - i].wait_recv()
+        for j in range(1, B):
+            c_axx[i, j] = remote(
+                aux.at[i, 0], aux.at[i, B - j], axx_s.at[i, j], axx_r.at[i, B - j], xpeer[j]
+            )
 
     for h in range(heads):
         cols = slice(h * hs, (h + 1) * hs)
         for s in range(R):
             ns[s, h] = decays[h] * st[s, h] + k_t[cols, s : s + 1] * v[s : s + 1, cols]
+
+    order = sorted(range(A), key=lambda i: min(i, A - i))
+    for i in order[1:]:
+        c_gz[A - i].wait_recv()
+        spread_block(i)
+        to_partner(i, 0)
 
     c_ext.wait_recv()
     for name in ("dg", "du", "dd", "eg0", "eu0", "eg1", "eu1", "ed1", "ed0"):
         local[name].wait()
     c_dg.wait_recv()
     c_du.wait_recv()
-
-    AR = A * R
+    group = max(1, min(A, ROWS // (B * R)))
+    rows = group * B * R
 
     def gate_row(ref):
         part = ref[...].astype(F32)
@@ -305,67 +302,83 @@
 
     gvec_o = gate_row(gate_vec)
     gvec_q = gate_row(gvec_p)
-
-    def ffn(j0, nj, slot):
-        rows = nj * AR
-        x_o = xo[j0 : j0 + nj].reshape(rows, H)
+    lanes = lax.broadcasted_iota(jnp.int32, (rows, 128), 1)
+    c_yx = {}
+    c_rx = {}
+    c_rz = {}
+
+    def arrive(i):
+        for j in range(1, B):
+            c_gx[i, B - j].wait_recv()
+            to_partner(i, j)
+
+    def experts(g):
+        slots = range(g * group, (g + 1) * group)
+        at = slice(g * group, (g + 1) * group)
+        for i in slots:
+            for j in range(1, B):
+                c_axx[i, B - j].wait_recv()
+        x_o = xo[at].reshape(rows, H)
         gate = dot_t(x_o, eg[0])
         up = dot_t(x_o, eu[0])
         d_gate = dot_t(x_o, dg[0])
         d_up = dot_t(x_o, du[0])
         logit = jnp.sum(x_o.astype(F32) * gvec_o, axis=1, keepdims=True)
-        for j in range(j0, j0 + nj):
-            for i in range(A):
-                c_gp[j, i].wait_recv()
-        x_p = xp[j0 : j0 + nj].reshape(rows, H)
+        for i in slots:
+            for j in range(B):
+                c_gp[i, j].wait_recv()
+        x_p = xp[at].reshape(rows, H)
         gate = gate + dot_t(x_p, eg[1])
         up = up + dot_t(x_p, eu[1])
         d_gate = d_gate + dot_t(x_p, dg[1])
         d_up = d_up + dot_t(x_p, du[1])
         logit = logit + jnp.sum(x_p.astype(F32) * gvec_q, axis=1, keepdims=True)
-        lanes = lax.broadcasted_iota(jnp.int32, (rows, 128), 1)
-        table = aux[j0 : j0 + nj].reshape(rows, 128).astype(F32)
+        table = aux[at].reshape(rows, 128).astype(F32)
         weight = jnp.sum(jnp.where(lanes == expert, table, 0.0), axis=1, keepdims=True)
         hidden = (silu(gate) * up).astype(BF16)
         d_hidden = (1.0 / (1.0 + jnp.exp(-logit)) * silu(d_gate) * d_up).astype(BF16)
-        yx_s[j0 : j0 + nj] = (weight * dot(hidden, ed[1])).astype(BF16).reshape(nj, A, R, H)
-        c_yx = remote(
-            yx_s.at[pl.ds(j0, nj)],
-            yx_r.at[pl.ds(j0, nj)],
-            yx_ss.at[slot],
-            yx_rs.at[slot],
-            partner,
-        )
+        yx_s[at] = (weight * dot(hidden, ed[1])).astype(BF16).reshape(group, B, R, H)
+        span = pl.ds(g * group, group)
+        c_yx[g] = remote(yx_s.at[span], yx_r.at[span], yx_ss.at[g], yx_rs.at[g], partner)
         y = weight * dot(hidden, ed[0]) + dot(d_hidden, dd[...])
-        c_yx.wait_recv()
-        return y.reshape(nj, A, R, H) + yx_r[j0 : j0 + nj].astype(F32)
-
-    y0[...] = ffn(0, 1, 0)[0]
-
-    for i in [0] + order:
-        for j in range(1, B):
-            c_gx[B - j, i].wait_recv()
-            to_partner(j, i)
-    for j in range(1, B):
-        c_axx[B - j].wait_recv()
-    group = max(g for g in range(1, B) if (B - 1) % g == 0 and (g * AR <= 256 or g == 1))
-    c_rx = [None] * B
-    for slot, j0 in enumerate(range(1, B, group)):
-        y = ffn(j0, group, slot + 1)
-        ys[j0 : j0 + group] = y.astype(BF16)
-        for j in range(j0, j0 + group):
-            c_rx[j] = remote(ys.at[j], rsx.at[B - j], rx_s.at[j], rx_r.at[B - j], xpeer[j])
-
-    total = y0[...]
-    for j in range(1, B):
-        c_rx[B - j].wait_recv()
-        total = total + rsx[j].astype(F32)
-    zs[...] = total.astype(BF16)
-    c_rz = [None] + [
-        remote(zs.at[i], rsz.at[A - i], rz_s.at[i], rz_r.at[A - i], zpeer[i])
-        for i in range(1, A)
-    ]
-    result = after + total[0]
+        y0[at] = y.reshape(group, B, R, H)
+
+    def plane_send(g):
+        c_yx[g].wait_recv()
+        for i in range(g * group, (g + 1) * group):
+            y = y0[i] + yx_r[i].astype(F32)
+            y0[i, 0] = y[0]
+            ys[i] = y.astype(BF16)
+            for j in range(1, B):
+                c_rx[i, j] = remote(
+                    ys.at[i, j], rsx.at[i, B - j], rx_s.at[i, j], rx_r.at[i, B - j], xpeer[j]
+                )
+
+    def plane_sum(g):
+        for i in range(g * group, (g + 1) * group):
+            total = y0[i, 0]
+            for j in range(1, B):
+                c_rx[i, B - j].wait_recv()
+                total = total + rsx[i, j].astype(F32)
+            if i == 0:
+                y0[0, 0] = total
+            else:
+                zs[i] = total.astype(BF16)
+                c_rz[i] = remote(zs.at[i], rsz.at[A - i], rz_s.at[i], rz_r.at[A - i], zpeer[i])
+
+    turns = A // group
+    for t in range(turns + 2):
+        if t < turns:
+            for i in order:
+                if i // group == t:
+                    arrive(i)
+            experts(t)
+        if 1 <= t <= turns:
+            plane_send(t - 1)
+        if t >= 2:
+            plane_sum(t - 2)
+
+    result = after + y0[0, 0]
     for i in range(1, A):
         c_rz[A - i].wait_recv()
         result = result + rsz[i].astype(F32)
@@ -464,14 +477,14 @@
             V(state.shape, F32),
             V((R, HW), BF16),
             V((R, HW), BF16),
-            V((B, A, R, 128), BF16),
-            V((B, A, R, H), BF16),
-            V((B, A, R, H), BF16),
-            V((A, R, H), F32),
-            V((B, A, R, H), BF16),
-            V((B, A, R, H), BF16),
-            V((B, A, R, H), BF16),
-            V((B, A, R, H), BF16),
+            V((A, B, R, 128), BF16),
+            V((A, B, R, H), BF16),
+            V((A, B, R, H), BF16),
+            V((A, B, R, H), F32),
+            V((A, B, R, H), BF16),
+            V((A, B, R, H), BF16),
+            V((A, B, R, H), BF16),
+            V((A, B, R, H), BF16),
             V((A, R, H), BF16),
             V((A, R, H), BF16),
             sem(25),
@@ -479,18 +492,18 @@
             sem(7),
             sem(A),
             sem(A),
-            sem(B),
-            sem(B),
-            sem(A),
-            sem(A),
-            sem(B, A),
-            sem(B, A),
-            sem(B, A),
-            sem(B, A),
-            sem(B),
-            sem(B),
-            sem(B),
-            sem(B),
+            sem(A, B),
+            sem(A, B),
+            sem(A),
+            sem(A),
+            sem(A, B),
+            sem(A, B),
+            sem(A, B),
+            sem(A, B),
+            sem(A),
+            sem(A),
+            sem(A, B),
+            sem(A, B),
             sem(A),
             sem(A),
         ],

time: 40.3 us -> 39.7 us (0.985)
  Pallas kernels: 39.5 us -> 39 us
    pallas_call x1, Pallas kernels: 38.1 us -> 37.6 us  [body(): pl.pallas_call(functools.partial(kernel, A, B), out_shape=(pltpu.VMEM((R,...]
where the time goes in v3:
time: 39.7 us; the launch traced here: 39.6 us
  Pallas kernels  39 us (98%)
  between operations  0.65 us (2%)
    pallas_call x1, Pallas kernels, body(): pl.pallas_call(functools.partial(kernel, A, B), out_shape=(pltpu.VMEM((R,...  37.6 us
    pallas_call x1, Pallas kernels, body(): pl.pallas_call(store, out_shape=(jax.ShapeDtypeStruct((R, H), BF16), jax....  1.34 us

profile of v3, /device:TPU:0, one launch (start us, length us, event | category | flops | bytes accessed | tf_op | source)
XLA Modules:
  0.0 39.6 jit_solution(7159313878068093703)
XLA Ops:
  0.6 37.6 %layer.1 = (bf16[16,1024]{1,0:T(8,128)(2,1)S(1)}, f32[16,2,128,128]{3,2,1,0:T(8,128)S(1)}) custom-call(bf16[16,1024]{1,0:T(8,128)(2,1)} %tokens_h.1, f32[1,2048]{1,0:T(1,128)} %bitcast.17, s32[2,16]{1,0:T(2,128)} %bitcast.20, bf16[2,16]{1,0:T(2,128)(2,1)} %bitcast.21, f32[1,1024]{1,0:T(1,128)} %bitcast.18, bf16[8,128]{1,0:T(8,128)(2,1)} %bitcast.19, ...), custom_call_target="tpu_custom_call" | custom-call | tf_op jit(solution)/shard_map/layer/pallas_call | solution.py:452
  38.3 1.3 %store.1 = (bf16[16,1024]{1,0:T(8,128)(2,1)}, f32[16,2,128,128]{3,2,1,0:T(8,128)}) custom-call(bf16[16,1024]{1,0:T(8,128)(2,1)S(1)} %get-tuple-element.4.a_in, f32[16,2,128,128]{3,2,1,0:T(8,128)S(1)} %get-tuple-element.5.b_in), custom_call_target="tpu_custom_call" | custom-call | tf_op jit(solution)/shard_map/store/pallas_call | solution.py:517
